TPU v7x, 32 devices: a whole 2x2x4 slice. The times are simulated.
32 devices in a mesh: dp: 4 (over y, x), kv: 4 (over z), tp: 2 (over core).
Axes of the slice: x: 2, y: 2, z: 4, core: 2. Of those that a mesh axis runs over, the one named last changes fastest.
Arguments:
- resid: bfloat16 [16, 2048], P('dp', ('kv', 'tp')), may hold values from -45 to 45
- norm_gain: bfloat16 [3, 2048], P(None, ('kv', 'tp')), may hold values from 0.099609375 to 1.8984375
- ffn_gate: bfloat16 [2, 2048, 5632], P(None, None, ('kv', 'tp')), may hold values from -0.125 to 0.125
- ffn_up: bfloat16 [2, 2048, 5632], P(None, None, ('kv', 'tp')), may hold values from -0.125 to 0.125
- ffn_down: bfloat16 [2, 5632, 2048], P(None, ('kv', 'tp')), may hold values from -0.109375 to 0.109375
- w_x: bfloat16 [2048, 64, 64], P(None, 'kv', 'tp'), may hold values from -0.125 to 0.125
- w_z: bfloat16 [2048, 64, 64], P(None, 'kv', 'tp'), may hold values from -0.125 to 0.125
- w_bc: bfloat16 [2048, 2, 8, 128], P('kv'), may hold values from -0.125 to 0.125
- w_dt: bfloat16 [2048, 64], P('kv'), may hold values from -0.125 to 0.125
- dt_bias: float32 [64], replicated, may hold values from -2 to 0.5
- a_log: float32 [64], replicated, may hold values from -1.5 to 1.5
- d_skip: float32 [64], replicated, may hold values from 0.5 to 1.5
- conv_wx: bfloat16 [4, 64, 64], P(None, None, 'tp'), may hold values from -3 to 3
- conv_wbc: bfloat16 [4, 2, 8, 128], replicated, may hold values from -3 to 3
- conv_x: bfloat16 [16, 3, 64, 64], P(('dp', 'kv'), None, None, 'tp'), may hold values from -6 to 6
- conv_bc: bfloat16 [16, 3, 2, 8, 128], P(('dp', 'kv')), may hold values from -6 to 6
- ssm_state: float32 [16, 64, 64, 128], P(('dp', 'kv'), None, 'tp'), may hold values from -3 to 3
- w_out: bfloat16 [64, 64, 2048], P(None, 'tp', 'kv'), may hold values from -0.09375 to 0.09375
Outputs:
- final: bfloat16 [16, 2048], P('dp', ('kv', 'tp'))
All inputs are finite; a program needn't handle non-finite values.
Results may differ from a plain program's by a relative error of at most 0.018.
Values may be sent and summed in bfloat16 or wider, within the bound.
No kernel may reach another device: no remote copies, remote signals or barrier semaphores. Data moves between devices by JAX's collectives and lax.ppermute only.
A program may use at most 64 MiB of HBM per device.

v0:
```python
import jax
import jax.numpy as jnp
from jax import lax
from jax.sharding import PartitionSpec as P

D = 2048
EPS = 1e-06


def normalize(rows, gain):
    values = rows.astype(jnp.float32)
    scale = lax.rsqrt(jnp.mean(values * values, axis=1, keepdims=True) + EPS)
    return (values * scale * gain.astype(jnp.float32).reshape(1, -1)).astype(jnp.bfloat16)


def feed_forward(normed, w_gate, w_up, w_down):
    gate = jnp.dot(normed, w_gate, preferred_element_type=jnp.float32)
    upper = jnp.dot(normed, w_up, preferred_element_type=jnp.float32)
    hidden = (jax.nn.silu(gate) * upper).astype(jnp.bfloat16)
    return jnp.dot(hidden, w_down, preferred_element_type=jnp.float32)


def add_half(base, sums):
    return (base.astype(jnp.float32) + 0.5 * sums).astype(jnp.bfloat16)


def ffn_totals(partial_value):
    return lax.psum(partial_value, ("kv", "tp"))


def short_conv(history, newest, taps):
    window = jnp.concatenate(
        [history.astype(jnp.float32), newest.astype(jnp.float32)[:, None]], axis=1
    )
    return jax.nn.silu(jnp.sum(window * taps.astype(jnp.float32)[None], axis=1))


def state_step(
    xs_new,
    zeta,
    bc_new,
    dt_raw,
    conv_x,
    conv_bc,
    ssm_state,
    conv_wx,
    conv_wbc,
    dt_bias,
    a_log,
    d_skip,
):
    xconv = short_conv(conv_x, xs_new, conv_wx)
    bconv = short_conv(conv_bc, bc_new, conv_wbc)
    heads = xconv.shape[1]
    groups = bconv.shape[2]
    bmat = jnp.repeat(bconv[:, 0], heads // groups, axis=1)
    cmat = jnp.repeat(bconv[:, 1], heads // groups, axis=1)
    step_size = jax.nn.softplus(dt_raw + dt_bias[None, :])
    decay = jnp.exp(-step_size * jnp.exp(a_log)[None, :])
    updated = (
        decay[:, :, None, None] * ssm_state
        + (step_size[:, :, None] * xconv)[..., None] * bmat[:, :, None, :]
    )
    mixed = (
        jnp.einsum("shpn,shn->shp", updated, cmat, precision=lax.Precision.HIGHEST)
        + d_skip[None, :, None] * xconv
    )
    return (mixed * jax.nn.silu(zeta.astype(jnp.float32))).astype(jnp.bfloat16)


def group_terms(slab, w_bc, w_dt):
    span = slab.shape[1]
    flat_bc = w_bc.reshape(span, -1)
    bc_part = jnp.dot(slab, flat_bc, preferred_element_type=jnp.float32)
    dt_part = jnp.dot(slab, w_dt, preferred_element_type=jnp.float32)
    return (
        lax.psum_scatter(bc_part, "kv", scatter_dimension=0, tiled=True),
        lax.psum_scatter(dt_part, "kv", scatter_dimension=0, tiled=True),
    )


def mix_partial(
    normed,
    w_x,
    w_z,
    w_bc,
    w_dt,
    dt_bias,
    a_log,
    d_skip,
    conv_wx,
    conv_wbc,
    conv_x,
    conv_bc,
    ssm_state,
    w_out,
):
    rows = normed.shape[0]
    local_heads = w_x.shape[1]
    half = w_x.shape[2]
    xs_part = (
        jnp.dot(normed, w_x.reshape(D, -1), preferred_element_type=jnp.float32)
        .astype(jnp.bfloat16)
        .reshape(rows, local_heads, half)
    )
    zeta_part = (
        jnp.dot(normed, w_z.reshape(D, -1), preferred_element_type=jnp.float32)
        .astype(jnp.bfloat16)
        .reshape(rows, local_heads, half)
    )
    xs_new, zeta = (
        lax.all_to_all(xs_part, "kv", split_axis=0, concat_axis=1, tiled=True),
        lax.all_to_all(zeta_part, "kv", split_axis=0, concat_axis=1, tiled=True),
    )
    span = w_bc.shape[0]
    slab = lax.dynamic_slice_in_dim(normed, lax.axis_index("kv") * span, span, 1)
    bc_sum, dt_raw = group_terms(slab, w_bc, w_dt)
    bc_new = bc_sum.astype(jnp.bfloat16).reshape((bc_sum.shape[0],) + w_bc.shape[1:])
    mixed = state_step(
        xs_new,
        zeta,
        bc_new,
        dt_raw,
        conv_x,
        conv_bc,
        ssm_state,
        conv_wx,
        conv_wbc,
        dt_bias,
        a_log,
        d_skip,
    )
    flat_out = w_out.reshape(-1, w_out.shape[2])
    piece = lax.all_gather(mixed, "kv", axis=0, tiled=True)
    return jnp.dot(piece.reshape(piece.shape[0], -1), flat_out, preferred_element_type=jnp.float32)


def per_device(
    resid,
    norm_gain,
    ffn_gate,
    ffn_up,
    ffn_down,
    w_x,
    w_z,
    w_bc,
    w_dt,
    dt_bias,
    a_log,
    d_skip,
    conv_wx,
    conv_wbc,
    conv_x,
    conv_bc,
    ssm_state,
    w_out,
):
    mixer_args = (
        w_x,
        w_z,
        w_bc,
        w_dt,
        dt_bias,
        a_log,
        d_skip,
        conv_wx,
        conv_wbc,
        conv_x,
        conv_bc,
        ssm_state,
        w_out,
    )
    rows, gains = (
        lax.all_gather(resid, ("kv", "tp"), axis=1, tiled=True),
        lax.all_gather(norm_gain, ("kv", "tp"), axis=1, tiled=True),
    )
    first = add_half(
        rows,
        ffn_totals(feed_forward(normalize(rows, gains[0]), ffn_gate[0], ffn_up[0], ffn_down[0])),
    )
    partial_value = mix_partial(normalize(first, gains[1]), *mixer_args)
    span = partial_value.shape[1]
    block = lax.dynamic_slice_in_dim(first, lax.axis_index("kv") * span, span, 1)
    joined = (block.astype(jnp.float32) + lax.psum(partial_value, "tp")).astype(jnp.bfloat16)
    second = lax.all_gather(joined, "kv", axis=1, tiled=True)
    final = add_half(
        second,
        ffn_totals(feed_forward(normalize(second, gains[2]), ffn_gate[1], ffn_up[1], ffn_down[1])),
    )
    width = resid.shape[1]
    return lax.dynamic_slice_in_dim(final, lax.axis_index(("kv", "tp")) * width, width, 1)


def solution(mesh):
    placed = (
        P("dp", ("kv", "tp")),
        P(None, ("kv", "tp")),
        P(None, None, ("kv", "tp")),
        P(None, None, ("kv", "tp")),
        P(None, ("kv", "tp"), None),
        P(None, "kv", "tp"),
        P(None, "kv", "tp"),
        P("kv", None, None, None),
        P("kv", None),
        P(),
        P(),
        P(),
        P(None, None, "tp"),
        P(),
        P(("dp", "kv"), None, None, "tp"),
        P(("dp", "kv"), None, None, None, None),
        P(("dp", "kv"), None, "tp", None),
        P(None, "tp", "kv"),
    )
    return jax.shard_map(
        per_device, mesh=mesh, in_specs=placed, out_specs=P("dp", ("kv", "tp")), check_vma=False
    )
```

profile of v0, /device:TPU:0, one launch (start us, length us, event | category | flops | bytes accessed | tf_op | source)
XLA Modules:
  0.0 168.5 jit_solution(16530086735748407296)
XLA Ops:
  0.0 14.7 %all_gather.12 = bf16[4,2048]{1,0:T(4,128)(2,1)S(1)} all-gather(bf16[4,256]{1,0:T(4,128)(2,1)} %param.18), channel_id=1, replica_groups=mesh['dp'=4,'kv'=4,'tp'=2] {'kv','tp'}, dimensions={1}, use_global_device_ids=true | all-gather | bytes 18432 | tf_op jit(solution)/shard_map/all_gather | solution.py:174
  14.7 0.1 fusion.48
  14.9 12.9 %all_gather.13 = bf16[3,2048]{1,0:T(4,128)(2,1)S(1)} all-gather(bf16[3,256]{1,0:T(4,128)(2,1)} %param.19), channel_id=1, replica_groups=mesh['dp'=4,'kv'=4,'tp'=2] {'kv','tp'}, dimensions={1}, use_global_device_ids=true | all-gather | bytes 13824 | tf_op jit(solution)/shard_map/all_gather | solution.py:175
  27.8 2.7 %fusion.10 = f32[4,704]{1,0:T(4,128)S(1)} fusion(bf16[2,2048,704]{1,2,0:T(8,128)(2,1)} %param.20, bf16[4,2048]{1,0:T(4,128)(2,1)S(1)} %all_gather.12, f32[2048]{0:T(1024)S(1)} %bitcast.113, f32[4]{0:T(128)S(1)} %add_rsqrt_fusion.2), kind=kOutput, calls=%fused_computation.10 | convolution fusion | flops 11567104 | bytes 2919440 | tf_op jit(solution)/shard_map/dot_general | solution.py:17
  30.5 4.4 %fusion.6 = f32[4,2048]{1,0:T(4,128)S(1)} fusion(bf16[2,704,2048]{2,1,0:T(8,128)(2,1)} %param.22, bf16[2,2048,704]{1,2,0:T(8,128)(2,1)} %param.21, f32[4,704]{1,0:T(4,128)S(1)} %fusion.10, bf16[4,2048]{1,0:T(4,128)(2,1)S(1)} %all_gather.12, f32[2048]{0:T(1024)S(1)} %bitcast.114, f32[4]{0:T(128)S(1)} %add_rsqrt_fusion.2), kind=kOutput, calls=%fused_computation.6 | convolution fusion | flops 23118336 | bytes 5835792 | tf_op jit(solution)/shard_map/dot_general | solution.py:20
  34.8 26.7 %psum.21 = f32[4,2048]{1,0:T(4,128)S(1)} all-reduce(f32[4,2048]{1,0:T(4,128)S(1)} %fusion.6), channel_id=1, replica_groups=mesh['dp'=4,'kv'=4,'tp'=2] {'kv','tp'}, use_global_device_ids=true, to_apply=%region_1.2 | all-reduce | flops 8192 | bytes 65536 | tf_op jit(solution)/shard_map/psum | solution.py:28
  61.5 0.1 fusion.45
  61.6 0.1 fusion.47
  61.7 0.0 copy-start.10
  61.7 0.0 copy-start.5
  61.8 0.0 copy-start.6
  61.8 0.0 copy-start.8
  61.8 0.0 copy-start.9
  61.8 0.6 convolution_convert_fusion.1
  62.4 0.0 copy-start.1
  62.5 0.1 reshape.198
  62.5 0.7 reshape.219
  63.2 3.2 %all-to-all-start = ((bf16[4,2,256]{2,1,0:T(2,128)(2,1)}), bf16[4,2,256]{2,1,0:T(2,128)(2,1)S(1)}, u32[]{:S(2)}, u32[]{:S(2)}) async-start(bf16[4,2,256]{2,1,0:T(2,128)(2,1)} %reshape.219), calls=%async_computation | async-start | bytes 8192 | tf_op jit(solution)/shard_map/all_to_all | solution.py:112
  66.5 0.0 copy-start.7
  66.5 2.2 %convolution_convert_fusion = bf16[4,512]{1,0:T(4,128)(2,1)S(1)} fusion(bf16[4,2048]{1,0:T(4,128)(2,1)S(1)} %fusion.47, bf16[2048,512]{0,1:T(8,128)(2,1)} %bitcast.109), kind=kOutput, calls=%fused_computation.26 | convolution fusion | flops 8390656 | bytes 2117632 | tf_op jit(solution)/shard_map/dot_general | solution.py:107
  68.7 0.1 fusion.69
  68.9 2.0 %fusion.18 = f32[4,2048]{1,0:T(4,128)S(1)} fusion(bf16[64,8,16,128]{3,2,1,0:T(8,128)(2,1)} %bitcast.108, bf16[4,2048]{1,0:T(4,128)(2,1)S(1)} %fusion.47, s32[]{:T(128)S(6)} %select_n.11), kind=kOutput, calls=%fused_computation.18 | convolution fusion | flops 8388608 | bytes 2134020 | tf_op jit(solution)/shard_map/dot_general | solution.py:74
  70.9 0.6 dynamic-slice
  71.4 19.8 %all-reduce.2 = (bf16[4,2048]{1,0:T(4,128)(2,1)S(1)}, f32[4,64]{1,0:T(4,128)S(1)}) all-reduce(f32[4,2048]{1,0:T(4,128)S(1)} %fusion.18, f32[4,64]{1,0:T(4,128)S(1)} %fusion.69), channel_id=4, replica_groups=mesh['dp'=4,'kv'=4,'tp'=2] {'kv'}, use_global_device_ids=true, to_apply=%region_5.6.clone | all-reduce | flops 8448 | bytes 51200
  91.2 0.7 fusion.60
  92.0 0.1 reshape.202
  92.1 0.7 reshape.217
  92.7 0.0 all-to-all-done
  92.8 3.2 %all-to-all-start.1 = ((bf16[4,2,256]{2,1,0:T(2,128)(2,1)}), bf16[4,2,256]{2,1,0:T(2,128)(2,1)S(1)}, u32[]{:S(2)}, u32[]{:S(2)}) async-start(bf16[4,2,256]{2,1,0:T(2,128)(2,1)} %reshape.217), calls=%async_computation.1 | async-start | bytes 8192 | tf_op jit(solution)/shard_map/all_to_all | solution.py:113
  96.0 0.7 fusion.75
  96.7 0.1 reshape.220
  96.8 0.1 copy.27
  96.9 4.7 %all-to-all-done.1 = bf16[4,2,256]{2,1,0:T(2,128)(2,1)S(1)} async-done(((bf16[4,2,256]{2,1,0:T(2,128)(2,1)}), bf16[4,2,256]{2,1,0:T(2,128)(2,1)S(1)}, u32[]{:S(2)}, u32[]{:S(2)}) %all-to-all-start.1) | async-done | bytes 4128 | tf_op jit(solution)/shard_map/all_to_all | solution.py:113
  101.6 0.1 reshape.218
  101.7 0.1 copy.30
  101.8 0.1 copy.28
  101.9 1.9 %fusion.33 = f32[64,1,32]{2,1,0:T(1,128)S(1)} fusion(f32[64,128,1]{1,2,0:T(1,128)S(1)} %bitcast.110, f32[1,64,32,128]{3,2,1,0:T(8,128)S(1)} %copy-done.1, f32[64,128]{1,0:T(8,128)S(1)} %broadcast_bitcast_fusion, f32[64,32]{1,0:T(8,128)S(1)} %copy.28, f32[64]{0:T(128)S(1)} %get-tuple-element.7), kind=kOutput, calls=%fused_computation.28 | convolution fusion | flops 3932160 | bytes 1130752 | tf_op jit(solution)/shard_map/shpn,shn->shp/dot_general | solution.py:65
  103.8 0.1 copy.34
  103.9 13.1 %all-gather.1 = bf16[4,64,32]{1,2,0:T(8,128)(2,1)S(1)} all-gather(bf16[1,64,32]{1,2,0:T(8,128)(2,1)S(1)} %fusion.64), channel_id=2, replica_groups=mesh['dp'=4,'kv'=4,'tp'=2] {'kv'}, dimensions={0}, use_global_device_ids=true | all-gather | bytes 20480 | tf_op jit(solution)/shard_map/all_gather | solution.py:134
  117.0 0.1 copy.35
  117.1 2.0 %convolution_bitcast_fusion = f32[4,512]{1,0:T(4,128)S(1)} fusion(bf16[4,64,32]{2,0,1:T(4,128)(2,1)S(1)} %copy.35, bf16[64,32,512]{2,1,0:T(8,128)(2,1)} %param.35), kind=kOutput, calls=%fused_computation.25 | convolution fusion | flops 8388608 | bytes 2121728 | tf_op jit(solution)/shard_map/dot_general | solution.py:135
  119.2 2.5 %psum.22 = f32[4,512]{1,0:T(4,128)S(1)} all-reduce(f32[4,512]{1,0:T(4,128)S(1)} %convolution_bitcast_fusion), channel_id=1, replica_groups=mesh['dp'=4,'kv'=4,'tp'=2] {'tp'}, use_global_device_ids=true, to_apply=%region_7.8 | all-reduce | flops 2048 | bytes 16384 | tf_op jit(solution)/shard_map/psum | solution.py:184
  121.6 13.2 %all_gather.15 = bf16[4,2048]{1,0:T(4,128)(2,1)S(1)} all-gather(bf16[4,512]{1,0:T(4,128)(2,1)S(1)} %add_convert_fusion), channel_id=1, replica_groups=mesh['dp'=4,'kv'=4,'tp'=2] {'kv'}, dimensions={1}, use_global_device_ids=true | all-gather | bytes 20480 | tf_op jit(solution)/shard_map/all_gather | solution.py:185
  134.8 0.1 multiply_reduce_fusion.1
  135.0 2.7 %fusion.4 = f32[4,704]{1,0:T(4,128)S(1)} fusion(bf16[2,2048,704]{1,2,0:T(8,128)(2,1)} %param.20, f32[2048]{0:T(1024)S(1)} %bitcast.111, f32[4]{0:T(128)S(1)} %add_rsqrt_fusion, bf16[4,2048]{1,0:T(4,128)(2,1)S(1)} %all_gather.15), kind=kOutput, calls=%fused_computation.4 | convolution fusion | flops 11567104 | bytes 2919440 | tf_op jit(solution)/shard_map/dot_general | solution.py:17
  137.7 4.4 %fusion = f32[4,2048]{1,0:T(4,128)S(1)} fusion(bf16[2,704,2048]{2,1,0:T(8,128)(2,1)} %param.22, bf16[2,2048,704]{1,2,0:T(8,128)(2,1)} %param.21, f32[4,704]{1,0:T(4,128)S(1)} %fusion.4, f32[2048]{0:T(1024)S(1)} %bitcast.112, f32[4]{0:T(128)S(1)} %add_rsqrt_fusion, bf16[4,2048]{1,0:T(4,128)(2,1)S(1)} %all_gather.15), kind=kOutput, calls=%fused_computation | convolution fusion | flops 23118336 | bytes 5835792 | tf_op jit(solution)/shard_map/dot_general | solution.py:20
  142.0 25.9 %psum.23 = f32[4,2048]{1,0:T(4,128)S(1)} all-reduce(f32[4,2048]{1,0:T(4,128)S(1)} %fusion), channel_id=1, replica_groups=mesh['dp'=4,'kv'=4,'tp'=2] {'kv','tp'}, use_global_device_ids=true, to_apply=%region_9.10 | all-reduce | flops 8192 | bytes 65536 | tf_op jit(solution)/shard_map/psum | solution.py:28
  168.0 0.6 fusion.67
  (30 shorter events, 0.2 us)
Async XLA Ops:
  0.0 61.7 %copy-start = (bf16[2048,16,32]{0,2,1:T(8,128)(2,1)S(1)}, bf16[2048,16,32]{0,2,1:T(8,128)(2,1)}, u32[]{:S(2)}) copy-start(bf16[2048,16,32]{0,2,1:T(8,128)(2,1)} %param.23) | copy-start | bytes 6291460
  34.8 33.9 %copy-start.2 = (bf16[512,64]{0,1:T(8,128)(2,1)S(1)}, bf16[512,64]{0,1:T(8,128)(2,1)}, u32[]{:S(2)}) copy-start(bf16[512,64]{0,1:T(8,128)(2,1)} %param.26) | copy-start | bytes 196612
  61.7 9.1 %copy-start.10 = (u32[32]{0:T(128)S(1)}, u32[32]{0:T(128)}, u32[]{:S(2)}) copy-start(u32[32]{0:T(128)} %constant.45) | copy-start | bytes 388
  61.7 30.2 %copy-start.5 = (bf16[4,2,8,128]{3,2,1,0:T(8,128)(2,1)S(1)}, bf16[4,2,8,128]{3,2,1,0:T(8,128)(2,1)}, u32[]{:S(2)}) copy-start(bf16[4,2,8,128]{3,2,1,0:T(8,128)(2,1)} %param.31) | copy-start | bytes 49156
  61.8 30.2 %copy-start.6 = (bf16[1,3,2,8,128]{4,3,2,1,0:T(8,128)(2,1)S(1)}, bf16[1,3,2,8,128]{4,3,2,1,0:T(8,128)(2,1)}, u32[]{:S(2)}) copy-start(bf16[1,3,2,8,128]{4,3,2,1,0:T(8,128)(2,1)} %param.33) | copy-start | bytes 36868
  61.8 34.2 %copy-start.8 = (f32[64]{0:T(128)S(1)}, f32[64]{0:T(128)}, u32[]{:S(2)}) copy-start(f32[64]{0:T(128)} %param.28) | copy-start | bytes 772
  61.8 34.2 %copy-start.9 = (f32[64]{0:T(128)S(1)}, f32[64]{0:T(128)}, u32[]{:S(2)}) copy-start(f32[64]{0:T(128)} %param.27) | copy-start | bytes 772
  62.4 39.3 %copy-start.3 = (bf16[4,64,32]{1,2,0:T(8,128)(2,1)S(1)}, bf16[4,64,32]{1,2,0:T(8,128)(2,1)}, u32[]{:S(2)}) copy-start(bf16[4,64,32]{1,2,0:T(8,128)(2,1)} %param.30) | copy-start | bytes 49156
  62.4 39.3 %copy-start.4 = (bf16[1,3,64,32]{2,3,1,0:T(8,128)(2,1)S(1)}, bf16[1,3,64,32]{2,3,1,0:T(8,128)(2,1)}, u32[]{:S(2)}) copy-start(bf16[1,3,64,32]{2,3,1,0:T(8,128)(2,1)} %param.32) | copy-start | bytes 36868
  62.4 39.4 %copy-start.1 = (f32[1,64,32,128]{3,2,1,0:T(8,128)S(1)}, f32[1,64,32,128]{3,2,1,0:T(8,128)}, u32[]{:S(2)}) copy-start(f32[1,64,32,128]{3,2,1,0:T(8,128)} %param.34) | copy-start | bytes 3145732
  63.2 29.5 %all-to-all-start = ((bf16[4,2,256]{2,1,0:T(2,128)(2,1)}), bf16[4,2,256]{2,1,0:T(2,128)(2,1)S(1)}, u32[]{:S(2)}, u32[]{:S(2)}) async-start(bf16[4,2,256]{2,1,0:T(2,128)(2,1)} %reshape.219), calls=%async_computation | async-start | bytes 8192 | tf_op jit(solution)/shard_map/all_to_all | solution.py:112
  66.5 37.4 %copy-start.7 = (f32[64]{0:T(128)S(1)}, f32[64]{0:T(128)}, u32[]{:S(2)}) copy-start(f32[64]{0:T(128)} %param.29) | copy-start | bytes 772
  92.8 8.8 %all-to-all-start.1 = ((bf16[4,2,256]{2,1,0:T(2,128)(2,1)}), bf16[4,2,256]{2,1,0:T(2,128)(2,1)S(1)}, u32[]{:S(2)}, u32[]{:S(2)}) async-start(bf16[4,2,256]{2,1,0:T(2,128)(2,1)} %reshape.217), calls=%async_computation.1 | async-start | bytes 8192 | tf_op jit(solution)/shard_map/all_to_all | solution.py:113
where the time goes:
time: 169 us
  blocking collectives  129 us (76%)
  matrix products  22.9 us (14%)
  starting transfers between devices  6.47 us (4%)
  waiting for transfers between devices  4.68 us (3%)
  local copies, waits for them, and re-layouts  3.47 us (2%)
  other arithmetic  1.89 us (1%)
    psum x2, blocking collectives, ffn_totals(): return lax.psum(partial_value, ('kv', 'tp'))  52.6 us
    unnamed x1, blocking collectives  19.8 us
    all_gather x1, blocking collectives, per_device(): lax.all_gather(resid, ('kv', 'tp'), axis=1, tiled=True)  14.7 us
    all_gather x1, blocking collectives, per_device(): second = lax.all_gather(joined, 'kv', axis=1, tiled=True)  13.2 us
    all_gather x1, blocking collectives, mix_partial(): piece = lax.all_gather(mixed, 'kv', axis=0, tiled=True)  13.1 us
    all_gather x1, blocking collectives, per_device(): lax.all_gather(norm_gain, ('kv', 'tp'), axis=1, tiled=True)  12.9 us
    dot_general x2, matrix products, feed_forward(): return jnp.dot(hidden, w_down, preferred_element_type=jnp.float32)  8.72 us
    dot_general x2, matrix products, feed_forward(): gate = jnp.dot(normed, w_gate, preferred_element_type=jnp.float32)  5.31 us
  transfers between devices with their start and end apart: 2, of which 1 were waited for; matrix products, arithmetic and copies ran while one was open for 4% of the time, Pallas kernels for 0%

commit v1 on v0

--- a/solution.py
+++ b/solution.py
@@ -182,7 +182,14 @@
     span = partial_value.shape[1]
     block = lax.dynamic_slice_in_dim(first, lax.axis_index("kv") * span, span, 1)
     joined = (block.astype(jnp.float32) + lax.psum(partial_value, "tp")).astype(jnp.bfloat16)
-    second = lax.all_gather(joined, "kv", axis=1, tiled=True)
+    peers = lax.axis_size("kv")
+    forward = [(i, (i + 1) % peers) for i in range(peers)]
+    parts = [joined]
+    for far in range(1, peers):
+        parts = [lax.ppermute(parts[0], "kv", forward), *parts]
+    whole = jnp.concatenate(parts, axis=1)
+    shift = (lax.axis_index("kv") + 1) * parts[-1].shape[1]
+    second = jnp.roll(whole, shift, axis=1)
     final = add_half(
         second,
         ffn_totals(feed_forward(normalize(second, gains[2]), ffn_gate[1], ffn_up[1], ffn_down[1])),

time: 169 us -> 172 us (1.018)
  waiting for transfers between devices: 4.68 us -> 20.9 us
  blocking collectives: 129 us -> 116 us
    ppermute x0 -> x3, waiting for transfers between devices: none -> 16.2 us  [per_device(): parts = [lax.ppermute(parts[0], 'kv', forward), *parts]]
    all_gather x1 -> x0, blocking collectives: 13.2 us -> none  [per_device(): second = lax.all_gather(joined, 'kv', axis=1, tiled=True)]
  transfers between devices with their start and end apart: 2 -> 5, of which waited for: 1 -> 4; matrix products, arithmetic and copies ran while one was open for 4% -> 4% of each run, Pallas kernels for 0% -> 0%
where the time goes in v1:
time: 172 us
  blocking collectives  116 us (67%)
  matrix products  22.9 us (13%)
  waiting for transfers between devices  20.9 us (12%)
  starting transfers between devices  6.53 us (4%)
  local copies, waits for them, and re-layouts  3.55 us (2%)
  other arithmetic  1.9 us (1%)
    psum x2, blocking collectives, ffn_totals(): return lax.psum(partial_value, ('kv', 'tp'))  52.6 us
    unnamed x1, blocking collectives  19.8 us
    ppermute x3, waiting for transfers between devices, per_device(): parts = [lax.ppermute(parts[0], 'kv', forward), *parts]  16.2 us
    all_gather x1, blocking collectives, per_device(): lax.all_gather(resid, ('kv', 'tp'), axis=1, tiled=True)  14.7 us
    all_gather x1, blocking collectives, mix_partial(): piece = lax.all_gather(mixed, 'kv', axis=0, tiled=True)  13.1 us
    all_gather x1, blocking collectives, per_device(): lax.all_gather(norm_gain, ('kv', 'tp'), axis=1, tiled=True)  12.9 us
    dot_general x2, matrix products, feed_forward(): return jnp.dot(hidden, w_down, preferred_element_type=jnp.float32)  8.72 us
    dot_general x2, matrix products, feed_forward(): gate = jnp.dot(normed, w_gate, preferred_element_type=jnp.float32)  5.32 us
  transfers between devices with their start and end apart: 5, of which 4 were waited for; matrix products, arithmetic and copies ran while one was open for 4% of the time, Pallas kernels for 0%

profile of v1, /device:TPU:0, one launch (start us, length us, event | category | flops | bytes accessed | tf_op | source)
XLA Modules:
  0.0 171.7 jit_solution(15846927619033325398)
XLA Ops:
  0.0 14.7 %all_gather.9 = bf16[4,2048]{1,0:T(4,128)(2,1)S(1)} all-gather(bf16[4,256]{1,0:T(4,128)(2,1)} %param.18), channel_id=1, replica_groups=mesh['dp'=4,'kv'=4,'tp'=2] {'kv','tp'}, dimensions={1}, use_global_device_ids=true | all-gather | bytes 18432 | tf_op jit(solution)/shard_map/all_gather | solution.py:174
  14.7 0.1 fusion.48
  14.9 12.9 %all_gather.10 = bf16[3,2048]{1,0:T(4,128)(2,1)S(1)} all-gather(bf16[3,256]{1,0:T(4,128)(2,1)} %param.19), channel_id=1, replica_groups=mesh['dp'=4,'kv'=4,'tp'=2] {'kv','tp'}, dimensions={1}, use_global_device_ids=true | all-gather | bytes 13824 | tf_op jit(solution)/shard_map/all_gather | solution.py:175
  27.8 2.7 %fusion.10 = f32[4,704]{1,0:T(4,128)S(1)} fusion(bf16[2,2048,704]{1,2,0:T(8,128)(2,1)} %param.20, bf16[4,2048]{1,0:T(4,128)(2,1)S(1)} %all_gather.9, f32[2048]{0:T(1024)S(1)} %bitcast.113, f32[4]{0:T(128)S(1)} %add_rsqrt_fusion.2), kind=kOutput, calls=%fused_computation.10 | convolution fusion | flops 11567104 | bytes 2919440 | tf_op jit(solution)/shard_map/dot_general | solution.py:17
  30.5 4.4 %fusion.6 = f32[4,2048]{1,0:T(4,128)S(1)} fusion(bf16[2,704,2048]{2,1,0:T(8,128)(2,1)} %param.22, bf16[2,2048,704]{1,2,0:T(8,128)(2,1)} %param.21, f32[4,704]{1,0:T(4,128)S(1)} %fusion.10, bf16[4,2048]{1,0:T(4,128)(2,1)S(1)} %all_gather.9, f32[2048]{0:T(1024)S(1)} %bitcast.114, f32[4]{0:T(128)S(1)} %add_rsqrt_fusion.2), kind=kOutput, calls=%fused_computation.6 | convolution fusion | flops 23118336 | bytes 5835792 | tf_op jit(solution)/shard_map/dot_general | solution.py:20
  34.8 26.7 %psum.21 = f32[4,2048]{1,0:T(4,128)S(1)} all-reduce(f32[4,2048]{1,0:T(4,128)S(1)} %fusion.6), channel_id=1, replica_groups=mesh['dp'=4,'kv'=4,'tp'=2] {'kv','tp'}, use_global_device_ids=true, to_apply=%region_1.2 | all-reduce | flops 8192 | bytes 65536 | tf_op jit(solution)/shard_map/psum | solution.py:28
  61.5 0.1 fusion.45
  61.6 0.1 fusion.47
  61.7 0.0 copy-start.10
  61.8 0.0 copy-start.6
  61.8 0.0 copy-start.8
  61.8 0.6 convolution_convert_fusion.1
  62.4 0.0 copy-start.1
  62.5 0.1 reshape.198
  62.5 0.7 reshape.219
  63.2 3.2 %all-to-all-start = ((bf16[4,2,256]{2,1,0:T(2,128)(2,1)}), bf16[4,2,256]{2,1,0:T(2,128)(2,1)S(1)}, u32[]{:S(2)}, u32[]{:S(2)}) async-start(bf16[4,2,256]{2,1,0:T(2,128)(2,1)} %reshape.219), calls=%async_computation | async-start | bytes 8192 | tf_op jit(solution)/shard_map/all_to_all | solution.py:112
  66.5 0.0 copy-start.7
  66.5 2.2 %convolution_convert_fusion = bf16[4,512]{1,0:T(4,128)(2,1)S(1)} fusion(bf16[4,2048]{1,0:T(4,128)(2,1)S(1)} %fusion.47, bf16[2048,512]{0,1:T(8,128)(2,1)} %bitcast.109), kind=kOutput, calls=%fused_computation.26 | convolution fusion | flops 8390656 | bytes 2117632 | tf_op jit(solution)/shard_map/dot_general | solution.py:107
  68.7 0.1 fusion.69
  68.9 2.0 %fusion.18 = f32[4,2048]{1,0:T(4,128)S(1)} fusion(bf16[64,8,16,128]{3,2,1,0:T(8,128)(2,1)} %bitcast.108, bf16[4,2048]{1,0:T(4,128)(2,1)S(1)} %fusion.47, s32[]{:T(128)S(6)} %select_n.24), kind=kOutput, calls=%fused_computation.18 | convolution fusion | flops 8388608 | bytes 2134020 | tf_op jit(solution)/shard_map/dot_general | solution.py:74
  70.9 0.6 dynamic-slice
  71.4 19.8 %all-reduce.2 = (bf16[4,2048]{1,0:T(4,128)(2,1)S(1)}, f32[4,64]{1,0:T(4,128)S(1)}) all-reduce(f32[4,2048]{1,0:T(4,128)S(1)} %fusion.18, f32[4,64]{1,0:T(4,128)S(1)} %fusion.69), channel_id=4, replica_groups=mesh['dp'=4,'kv'=4,'tp'=2] {'kv'}, use_global_device_ids=true, to_apply=%region_5.6.clone | all-reduce | flops 8448 | bytes 51200
  91.2 0.7 fusion.60
  92.0 0.1 reshape.202
  92.1 0.7 reshape.217
  92.8 3.2 %all-to-all-start.1 = ((bf16[4,2,256]{2,1,0:T(2,128)(2,1)}), bf16[4,2,256]{2,1,0:T(2,128)(2,1)S(1)}, u32[]{:S(2)}, u32[]{:S(2)}) async-start(bf16[4,2,256]{2,1,0:T(2,128)(2,1)} %reshape.217), calls=%async_computation.1 | async-start | bytes 8192 | tf_op jit(solution)/shard_map/all_to_all | solution.py:113
  96.0 0.7 fusion.75
  96.7 0.1 reshape.220
  96.8 0.1 copy.27
  96.9 4.7 %all-to-all-done.1 = bf16[4,2,256]{2,1,0:T(2,128)(2,1)S(1)} async-done(((bf16[4,2,256]{2,1,0:T(2,128)(2,1)}), bf16[4,2,256]{2,1,0:T(2,128)(2,1)S(1)}, u32[]{:S(2)}, u32[]{:S(2)}) %all-to-all-start.1) | async-done | bytes 4128 | tf_op jit(solution)/shard_map/all_to_all | solution.py:113
  101.6 0.1 reshape.218
  101.7 0.1 copy.30
  101.8 0.1 copy.28
  101.9 1.9 %fusion.33 = f32[64,1,32]{2,1,0:T(1,128)S(1)} fusion(f32[64,128,1]{1,2,0:T(1,128)S(1)} %bitcast.110, f32[1,64,32,128]{3,2,1,0:T(8,128)S(1)} %copy-done.1, f32[64,128]{1,0:T(8,128)S(1)} %broadcast_bitcast_fusion, f32[64,32]{1,0:T(8,128)S(1)} %copy.28, f32[64]{0:T(128)S(1)} %get-tuple-element.7), kind=kOutput, calls=%fused_computation.28 | convolution fusion | flops 3932160 | bytes 1130752 | tf_op jit(solution)/shard_map/shpn,shn->shp/dot_general | solution.py:65
  103.8 0.1 copy.34
  103.9 13.1 %all-gather.1 = bf16[4,64,32]{1,2,0:T(8,128)(2,1)S(1)} all-gather(bf16[1,64,32]{1,2,0:T(8,128)(2,1)S(1)} %fusion.64), channel_id=2, replica_groups=mesh['dp'=4,'kv'=4,'tp'=2] {'kv'}, dimensions={0}, use_global_device_ids=true | all-gather | bytes 20480 | tf_op jit(solution)/shard_map/all_gather | solution.py:134
  117.0 0.1 copy.35
  117.1 2.0 %convolution_bitcast_fusion = f32[4,512]{1,0:T(4,128)S(1)} fusion(bf16[4,64,32]{2,0,1:T(4,128)(2,1)S(1)} %copy.35, bf16[64,32,512]{2,1,0:T(8,128)(2,1)} %param.35), kind=kOutput, calls=%fused_computation.25 | convolution fusion | flops 8388608 | bytes 2121728 | tf_op jit(solution)/shard_map/dot_general | solution.py:135
  119.2 2.5 %psum.22 = f32[4,512]{1,0:T(4,128)S(1)} all-reduce(f32[4,512]{1,0:T(4,128)S(1)} %convolution_bitcast_fusion), channel_id=1, replica_groups=mesh['dp'=4,'kv'=4,'tp'=2] {'tp'}, use_global_device_ids=true, to_apply=%region_7.8 | all-reduce | flops 2048 | bytes 16384 | tf_op jit(solution)/shard_map/psum | solution.py:184
  121.6 0.1 collective-permute-start
  121.7 5.4 %collective-permute-done = bf16[4,512]{1,0:T(4,128)(2,1)S(1)} collective-permute-done((bf16[4,512]{1,0:T(4,128)(2,1)S(1)}, bf16[4,512]{1,0:T(4,128)(2,1)S(1)}, u32[]{:S(2)}, u32[]{:S(2)}) %collective-permute-start) | collective-permute-done | bytes 4128 | tf_op jit(solution)/shard_map/ppermute | solution.py:189
  127.1 5.4 %collective-permute-done.1 = bf16[4,512]{1,0:T(4,128)(2,1)S(1)} collective-permute-done((bf16[4,512]{1,0:T(4,128)(2,1)S(1)}, bf16[4,512]{1,0:T(4,128)(2,1)S(1)}, u32[]{:S(2)}, u32[]{:S(2)}) %collective-permute-start.1) | collective-permute-done | bytes 4128 | tf_op jit(solution)/shard_map/ppermute | solution.py:189
  132.5 5.4 %collective-permute-done.2 = bf16[4,512]{1,0:T(4,128)(2,1)S(1)} collective-permute-done((bf16[4,512]{1,0:T(4,128)(2,1)S(1)}, bf16[4,512]{1,0:T(4,128)(2,1)S(1)}, u32[]{:S(2)}, u32[]{:S(2)}) %collective-permute-start.2) | collective-permute-done | bytes 4128 | tf_op jit(solution)/shard_map/ppermute | solution.py:189
  138.0 0.1 multiply_reduce_fusion.1
  138.2 2.7 %fusion.4 = f32[4,704]{1,0:T(4,128)S(1)} fusion(bf16[2,2048,704]{1,2,0:T(8,128)(2,1)} %param.20, f32[2048]{0:T(1024)S(1)} %bitcast.111, f32[4]{0:T(128)S(1)} %add_rsqrt_fusion, bf16[4,4096]{1,0:T(4,128)(2,1)S(1)} %constant_dynamic-update-slice_fusion, s32[]{:T(128)S(6)} %select_n.27), kind=kOutput, calls=%fused_computation.4 | convolution fusion | flops 11567104 | bytes 2919940 | tf_op jit(solution)/shard_map/dot_general | solution.py:17
  140.8 4.4 %fusion = f32[4,2048]{1,0:T(4,128)S(1)} fusion(bf16[2,704,2048]{2,1,0:T(8,128)(2,1)} %param.22, bf16[2,2048,704]{1,2,0:T(8,128)(2,1)} %param.21, f32[4,704]{1,0:T(4,128)S(1)} %fusion.4, f32[2048]{0:T(1024)S(1)} %bitcast.112, f32[4]{0:T(128)S(1)} %add_rsqrt_fusion, bf16[4,4096]{1,0:T(4,128)(2,1)S(1)} %constant_dynamic-update-slice_fusion, s32[]{:T(128)S(6)} %select_n.27), kind=kOutput, calls=%fused_computation | convolution fusion | flops 23118336 | bytes 5837316 | tf_op jit(solution)/shard_map/dot_general | solution.py:20
  145.2 25.9 %psum.23 = f32[4,2048]{1,0:T(4,128)S(1)} all-reduce(f32[4,2048]{1,0:T(4,128)S(1)} %fusion), channel_id=1, replica_groups=mesh['dp'=4,'kv'=4,'tp'=2] {'kv','tp'}, use_global_device_ids=true, to_apply=%region_9.10 | all-reduce | flops 8192 | bytes 65536 | tf_op jit(solution)/shard_map/psum | solution.py:28
  171.1 0.6 fusion.67
  (43 shorter events, 0.3 us)
Async XLA Ops:
  0.0 61.7 %copy-start = (bf16[2048,16,32]{0,2,1:T(8,128)(2,1)S(1)}, bf16[2048,16,32]{0,2,1:T(8,128)(2,1)}, u32[]{:S(2)}) copy-start(bf16[2048,16,32]{0,2,1:T(8,128)(2,1)} %param.23) | copy-start | bytes 6291460
  34.8 33.9 %copy-start.2 = (bf16[512,64]{0,1:T(8,128)(2,1)S(1)}, bf16[512,64]{0,1:T(8,128)(2,1)}, u32[]{:S(2)}) copy-start(bf16[512,64]{0,1:T(8,128)(2,1)} %param.26) | copy-start | bytes 196612
  61.7 9.1 %copy-start.10 = (u32[32]{0:T(128)S(1)}, u32[32]{0:T(128)}, u32[]{:S(2)}) copy-start(u32[32]{0:T(128)} %constant.67) | copy-start | bytes 388
  61.7 30.2 %copy-start.5 = (bf16[4,2,8,128]{3,2,1,0:T(8,128)(2,1)S(1)}, bf16[4,2,8,128]{3,2,1,0:T(8,128)(2,1)}, u32[]{:S(2)}) copy-start(bf16[4,2,8,128]{3,2,1,0:T(8,128)(2,1)} %param.31) | copy-start | bytes 49156
  61.8 30.2 %copy-start.6 = (bf16[1,3,2,8,128]{4,3,2,1,0:T(8,128)(2,1)S(1)}, bf16[1,3,2,8,128]{4,3,2,1,0:T(8,128)(2,1)}, u32[]{:S(2)}) copy-start(bf16[1,3,2,8,128]{4,3,2,1,0:T(8,128)(2,1)} %param.33) | copy-start | bytes 36868
  61.8 34.2 %copy-start.8 = (f32[64]{0:T(128)S(1)}, f32[64]{0:T(128)}, u32[]{:S(2)}) copy-start(f32[64]{0:T(128)} %param.28) | copy-start | bytes 772
  61.8 34.2 %copy-start.9 = (f32[64]{0:T(128)S(1)}, f32[64]{0:T(128)}, u32[]{:S(2)}) copy-start(f32[64]{0:T(128)} %param.27) | copy-start | bytes 772
  62.4 39.3 %copy-start.3 = (bf16[4,64,32]{1,2,0:T(8,128)(2,1)S(1)}, bf16[4,64,32]{1,2,0:T(8,128)(2,1)}, u32[]{:S(2)}) copy-start(bf16[4,64,32]{1,2,0:T(8,128)(2,1)} %param.30) | copy-start | bytes 49156
  62.4 39.3 %copy-start.4 = (bf16[1,3,64,32]{2,3,1,0:T(8,128)(2,1)S(1)}, bf16[1,3,64,32]{2,3,1,0:T(8,128)(2,1)}, u32[]{:S(2)}) copy-start(bf16[1,3,64,32]{2,3,1,0:T(8,128)(2,1)} %param.32) | copy-start | bytes 36868
  62.4 39.4 %copy-start.1 = (f32[1,64,32,128]{3,2,1,0:T(8,128)S(1)}, f32[1,64,32,128]{3,2,1,0:T(8,128)}, u32[]{:S(2)}) copy-start(f32[1,64,32,128]{3,2,1,0:T(8,128)} %param.34) | copy-start | bytes 3145732
  63.2 29.5 %all-to-all-start = ((bf16[4,2,256]{2,1,0:T(2,128)(2,1)}), bf16[4,2,256]{2,1,0:T(2,128)(2,1)S(1)}, u32[]{:S(2)}, u32[]{:S(2)}) async-start(bf16[4,2,256]{2,1,0:T(2,128)(2,1)} %reshape.219), calls=%async_computation | async-start | bytes 8192 | tf_op jit(solution)/shard_map/all_to_all | solution.py:112
  66.5 37.4 %copy-start.7 = (f32[64]{0:T(128)S(1)}, f32[64]{0:T(128)}, u32[]{:S(2)}) copy-start(f32[64]{0:T(128)} %param.29) | copy-start | bytes 772
  92.8 8.8 %all-to-all-start.1 = ((bf16[4,2,256]{2,1,0:T(2,128)(2,1)}), bf16[4,2,256]{2,1,0:T(2,128)(2,1)S(1)}, u32[]{:S(2)}, u32[]{:S(2)}) async-start(bf16[4,2,256]{2,1,0:T(2,128)(2,1)} %reshape.217), calls=%async_computation.1 | async-start | bytes 8192 | tf_op jit(solution)/shard_map/all_to_all | solution.py:113
  121.6 5.5 %collective-permute-start = (bf16[4,512]{1,0:T(4,128)(2,1)S(1)}, bf16[4,512]{1,0:T(4,128)(2,1)S(1)}, u32[]{:S(2)}, u32[]{:S(2)}) collective-permute-start(bf16[4,512]{1,0:T(4,128)(2,1)S(1)} %add_convert_fusion), channel_id=1, source_target_pairs={{0,2},{2,4},{4,6},{6,0},{1,3},{3,5},{5,7},{7,1},{8,10},{10,12},{12... | collective-permute-start | bytes 12296 | tf_op jit(solution)/shard_map/ppermute | solution.py:189
  127.1 5.4 %collective-permute-start.1 = (bf16[4,512]{1,0:T(4,128)(2,1)S(1)}, bf16[4,512]{1,0:T(4,128)(2,1)S(1)}, u32[]{:S(2)}, u32[]{:S(2)}) collective-permute-start(bf16[4,512]{1,0:T(4,128)(2,1)S(1)} %collective-permute-done), channel_id=1, source_target_pairs={{0,2},{2,4},{4,6},{6,0},{1,3},{3,5},{5,7},{7,1},{8,10},{10,12},{12... | collective-permute-start | bytes 12296 | tf_op jit(solution)/shard_map/ppermute | solution.py:189
  132.5 5.4 %collective-permute-start.2 = (bf16[4,512]{1,0:T(4,128)(2,1)S(1)}, bf16[4,512]{1,0:T(4,128)(2,1)S(1)}, u32[]{:S(2)}, u32[]{:S(2)}) collective-permute-start(bf16[4,512]{1,0:T(4,128)(2,1)S(1)} %collective-permute-done.1), channel_id=1, source_target_pairs={{0,2},{2,4},{4,6},{6,0},{1,3},{3,5},{5,7},{7,1},{8,10},{10,12},{12... | collective-permute-start | bytes 12296 | tf_op jit(solution)/shard_map/ppermute | solution.py:189
